TPU v7x, 32 devices: a whole 2x2x4 slice. The times are simulated.
32 devices in a mesh: grp: 2 (over y), fs: 8 (over z, core), tp: 2 (over x).
Axes of the slice: x: 2, y: 2, z: 4, core: 2. Of those that a mesh axis runs over, the one named last changes fastest.
Arguments:
- prompt: bfloat16 [6144, 2048], P(('grp', 'fs')), parts along dimension 0, may hold values from -6 to 6
- routes: int32 [6144, 4], P(('grp', 'fs')), parts along dimension 0, may hold values from 0 to 7, all different within a row; in each aligned block of 384 rows (0 to 383, 384 to 767, ...) at most 240 rows name the same one
- route_weight: float32 [6144, 4], P(('grp', 'fs')), parts along dimension 0, may hold values from 0.2 to 1
- norm_gain: float32 [2048], P('fs'), may hold values from 0.1 to 1.9
- gate_train: float32 [8, 2048, 1024], P(None, 'fs', 'tp'), may hold values from -0.4 to 0.4
- up_train: float32 [8, 2048, 1024], P(None, 'fs', 'tp'), may hold values from -0.4 to 0.4
- down_train: float32 [8, 1024, 2048], P(None, 'fs', 'tp'), may hold values from -0.07 to 0.07
Outputs:
- gate_serve: bfloat16 [16, 2048, 1024], P(('grp', 'fs'), None, 'tp'), parts along dimension 0
- up_serve: bfloat16 [16, 2048, 1024], P(('grp', 'fs'), None, 'tp'), parts along dimension 0
- down_serve: bfloat16 [16, 1024, 2048], P(('grp', 'fs'), 'tp'), parts along dimension 0
- mixed: bfloat16 [6144, 2048], P(('grp', 'fs'), 'tp'), parts along dimension 0
There are 2 independent parts, one for each index of `grp`. A program takes and returns all parts, laid end to end along the dimension named above; an argument that names none is the same for every part. Nothing has to cross between parts.
Inputs may be any that keep to these rules, and one draw needn't show every extreme that they name: `routes`: each row names 4 different experts. Among the rows of one index of fs no expert is named more than 240 times, a bound that some block reaches on some index.
All inputs are finite; a program needn't handle non-finite values.
Results may differ from a plain program's by a relative error of at most 0.012.
Values may be sent and summed in bfloat16 or wider, within the bound.
No kernel may reach another device: no remote copies, remote signals or barrier semaphores. Data moves between devices by JAX's collectives and lax.ppermute only.
A program may use at most 128 MiB of HBM per device.

v0:
```python
import jax
import jax.numpy as jnp
from jax import lax
from jax.sharding import PartitionSpec as P

TOP = 4
LIMIT = 7.0
ALPHA = 1.702
EPS = 1e-06


def shards(prompt, routes, route_weight, norm_gain, gate_train, up_train, down_train):
    gate_cast = (norm_gain[None, :, None] * gate_train).astype(jnp.bfloat16)
    up_cast = (norm_gain[None, :, None] * up_train).astype(jnp.bfloat16)
    down_cast = down_train.astype(jnp.bfloat16)
    gate_mine, up_mine = (
        lax.all_to_all(gate_cast, "fs", split_axis=0, concat_axis=1, tiled=True),
        lax.all_to_all(up_cast, "fs", split_axis=0, concat_axis=1, tiled=True),
    )
    down_rows = lax.all_to_all(down_cast, "fs", split_axis=0, concat_axis=1, tiled=True)
    down_mine = lax.all_to_all(down_rows, "tp", split_axis=1, concat_axis=2, tiled=True)
    tok_rows, width = prompt.shape
    experts = gate_train.shape[0]
    quarter = width // lax.axis_size("tp")
    capacity = min(tok_rows, max(2, 5 * tok_rows * TOP // (4 * experts)))
    values = prompt.astype(jnp.float32)
    normed = (values * lax.rsqrt(jnp.mean(values * values, axis=-1, keepdims=True) + EPS)).astype(
        jnp.bfloat16
    )
    flat_expert = routes.reshape(-1)
    onehot = (flat_expert[:, None] == jnp.arange(experts, dtype=jnp.int32)[None, :]).astype(
        jnp.int32
    )
    earlier = jnp.cumsum(onehot, axis=0) - onehot
    slot_pos = jnp.sum(earlier * onehot, axis=1)
    target = flat_expert * capacity + slot_pos
    source_row = jnp.arange(tok_rows * TOP, dtype=jnp.int32) // TOP
    outbox = jnp.zeros((experts * capacity, width), jnp.bfloat16).at[target].set(normed[source_row])
    inbox = lax.all_to_all(
        outbox.reshape(experts, capacity, width), "fs", split_axis=0, concat_axis=1, tiled=True
    )
    gate_pre = jnp.einsum("erd,edf->erf", inbox, gate_mine, preferred_element_type=jnp.float32)
    up_pre = jnp.einsum("erd,edf->erf", inbox, up_mine, preferred_element_type=jnp.float32)
    gate_pre = jnp.minimum(gate_pre, LIMIT)
    up_pre = jnp.clip(up_pre, -LIMIT, LIMIT)
    hidden = ((up_pre + 1.0) * gate_pre * jax.nn.sigmoid(ALPHA * gate_pre)).astype(jnp.bfloat16)
    own_width = hidden.shape[2]
    empty = jnp.zeros((hidden.shape[0], hidden.shape[1], down_rows.shape[2]), jnp.float32)
    total = empty
    piece = lax.all_gather(hidden, "tp", axis=2, tiled=True)
    for index in range(piece.shape[2] // own_width):
        cols = piece[:, :, index * own_width : (index + 1) * own_width]
        weight_rows = lax.dynamic_slice_in_dim(down_rows, index * own_width, own_width, 1)
        part = jnp.einsum(
            "erf,efd->erd", cols, weight_rows, preferred_element_type=jnp.float32
        ).astype(jnp.bfloat16)
        total = total + part.astype(jnp.float32)
    summed = total.astype(jnp.bfloat16)
    back = lax.all_to_all(summed, "fs", split_axis=1, concat_axis=0, tiled=True)
    picked = back.reshape(experts * capacity, quarter)[target].astype(jnp.float32)
    weighted = picked.reshape(tok_rows, TOP, quarter) * route_weight[:, :, None]
    mixed = jnp.sum(weighted, axis=1).astype(jnp.bfloat16)
    return (gate_mine, up_mine, down_mine, mixed)


def solution(mesh):
    return jax.shard_map(
        shards,
        mesh=mesh,
        in_specs=(
            P(("grp", "fs"), None),
            P(("grp", "fs"), None),
            P(("grp", "fs"), None),
            P("fs"),
            P(None, "fs", "tp"),
            P(None, "fs", "tp"),
            P(None, "fs", "tp"),
        ),
        out_specs=(
            P(("grp", "fs"), None, "tp"),
            P(("grp", "fs"), None, "tp"),
            P(("grp", "fs"), "tp", None),
            P(("grp", "fs"), "tp"),
        ),
        check_vma=False,
    )
```

profile of v0, /device:TPU:0, one launch (start us, length us, event | category | flops | bytes accessed | tf_op | source)
XLA Modules:
  0.0 601.2 jit_solution(9907944391653193153)
XLA Ops:
  7.2 6.8 %multiply_convert_fusion = (bf16[8,256,512]{2,1,0:T(8,128)(2,1)}, bf16[8,256,512]{2,1,0:T(8,128)(2,1)}) fusion(f32[8,256,512]{2,1,0:T(8,128)} %param.12, f32[256]{0:T(256)} %param.10, f32[8,256,512]{2,1,0:T(8,128)} %param.11), kind=kLoop, calls=%fused_computation.7 | loop fusion | flops 4194304 | bytes 12583936 | tf_op jit(solution)/shard_map/convert_element_type | solution.py:14
  14.0 6.5 %all-to-all-start = ((bf16[8,256,512]{2,1,0:T(8,128)(2,1)}), bf16[8,256,512]{2,1,0:T(8,128)(2,1)S(1)}, u32[]{:S(2)}, u32[]{:S(2)}) async-start(bf16[8,256,512]{2,1,0:T(8,128)(2,1)} %get-tuple-element.17), calls=%async_computation | async-start | bytes 4194304 | tf_op jit(solution)/shard_map/all_to_all | solution.py:17
  20.5 0.1 copy.32
  20.6 0.1 eq.29
  20.8 0.1 eq.25
  20.9 2.3 reduce-window.6
  23.2 0.3 slice_reduce_fusion
  23.5 0.2 reduce-window.9
  23.7 0.1 copy.31
  23.8 0.2 mul.72
  24.0 0.6 fusion.12
  24.6 0.1 add_bitcast_fusion
  24.7 1.8 fusion.4
  26.5 2.9 fusion.5
  29.4 33.0 %scatter_custom_fusion = bf16[1920,2048]{1,0:T(8,128)(2,1)} fusion(s32[1536]{0:T(1024)S(1)} %fusion.11, bf16[384,2048]{1,0:T(8,128)(2,1)} %fusion.5, s32[2048]{0:T(1024)S(1)} %pad_clamp_fusion.1, bf16[]{:T(256)} %constant.17.clone.1), kind=kCustom, calls=%fused_computation.4 | custom fusion | bytes 7864832 | tf_op jit(solution)/shard_map/scatter | solution.py:38
  62.4 7.1 %all-to-all-done = bf16[8,256,512]{2,1,0:T(8,128)(2,1)S(1)} async-done(((bf16[8,256,512]{2,1,0:T(8,128)(2,1)}), bf16[8,256,512]{2,1,0:T(8,128)(2,1)S(1)}, u32[]{:S(2)}, u32[]{:S(2)}) %all-to-all-start) | async-done | bytes 2097184 | tf_op jit(solution)/shard_map/all_to_all | solution.py:17
  69.5 178.2 %all_to_all.72 = bf16[8,240,2048]{2,1,0:T(8,128)(2,1)} all-to-all(bf16[8,240,2048]{2,1,0:T(8,128)(2,1)} %bitcast.61), channel_id=1, replica_groups=mesh['grp'=2,'fs'=8,'tp'=2] {'fs'}, dimensions={0} | all-to-all | bytes 15728640 | tf_op jit(solution)/shard_map/all_to_all | solution.py:39
  247.7 4.4 all-to-all-start.1
  252.1 9.5 %fusion.13 = f32[1920,512]{1,0:T(8,128)} fusion(bf16[1920,2048]{1,0:T(8,128)(2,1)} %bitcast.73, bf16[2048,512]{1,0:T(8,128)(2,1)S(1)} %bitcast.70), kind=kOutput, calls=%fused_computation.45 | convolution fusion | flops 4026531840 | bytes 13893632 | tf_op jit(solution)/shard_map/erd,edf->erf/dot_general | solution.py:42
  261.6 39.5 %all-to-all-done.1 = bf16[8,256,512]{2,1,0:T(8,128)(2,1)} async-done(((bf16[8,256,512]{2,1,0:T(8,128)(2,1)}), bf16[8,256,512]{2,1,0:T(8,128)(2,1)}, u32[]{:S(2)}, u32[]{:S(2)}) %all-to-all-start.1) | async-done | bytes 2097184 | tf_op jit(solution)/shard_map/all_to_all | solution.py:18
  301.1 11.8 %multiply_convert_fusion.2 = bf16[1920,512]{1,0:T(8,128)(2,1)} fusion(f32[1920,512]{1,0:T(8,128)} %fusion.13, bf16[1920,2048]{1,0:T(8,128)(2,1)} %bitcast.74, bf16[2048,512]{1,0:T(8,128)(2,1)} %bitcast.8), kind=kOutput, calls=%fused_computation.11 | convolution fusion | flops 4036362240 | bytes 15859712 | tf_op jit(solution)/shard_map/erd,edf->erf/dot_general | solution.py:43
  312.9 2.5 convert_element_type.62
  315.4 51.7 %all_to_all.73 = bf16[8,128,1024]{2,1,0:T(8,128)(2,1)S(1)} all-to-all(bf16[8,128,1024]{2,1,0:T(8,128)(2,1)S(1)} %convert_element_type.62), channel_id=1, replica_groups=mesh['grp'=2,'fs'=8,'tp'=2] {'fs'}, dimensions={0} | all-to-all | bytes 4194304 | tf_op jit(solution)/shard_map/all_to_all | solution.py:20
  367.1 1.3 copy-done
  368.4 5.2 copy.46
  373.6 0.5 broadcast.146
  374.1 12.8 %reduce.6 = bf16[1024,1024]{1,0:T(8,128)(2,1)S(1)} reduce(bf16[1024,1,1024]{2,1,0:T(2,128)(2,1)} %bitcast.64, bf16[]{:T(256)} %broadcast.146), dimensions={1}, to_apply=%bitcast.58.reduce_sub_computation | reduce | bytes 4194306
  386.9 2.5 reshape.227
  389.4 4.2 all-to-all-start.3
  393.6 4.2 fusion.6
  397.8 2.3 fusion.2
  400.1 27.0 %copy.45 = bf16[1,1920,1024]{2,0,1:T(2,128)(2,1)} copy(bf16[1,1920,1024]{2,1,0:T(8,128)(2,1)S(1)} %fusion.2) | data formatting | bytes 7864320 | tf_op jit(solution)/shard_map/convert_element_type | solution.py:58
  427.1 24.6 %reduce.7 = bf16[1920,1024]{1,0:T(8,128)(2,1)} reduce(bf16[1920,1,1024]{2,1,0:T(2,128)(2,1)} %bitcast.62, bf16[]{:T(256)} %broadcast.146), dimensions={1}, to_apply=%bitcast.57.reduce_sub_computation | reduce | bytes 7864322
  451.7 7.6 %reshape.225 = bf16[8,2,122880]{2,1,0:T(2,128)(2,1)} reshape(bf16[1920,1024]{1,0:T(8,128)(2,1)} %reduce.7) | data formatting | bytes 7864320
  459.3 4.8 all-to-all-start.5
  464.2 0.1 copy.35
  464.3 3.1 reshape.228
  467.4 3.0 copy.37
  470.4 2.6 copy.30
  473.0 3.9 copy.36
  476.9 75.6 %all-to-all-done.5 = bf16[8,2,122880]{2,1,0:T(2,128)(2,1)} async-done(((bf16[8,2,122880]{2,1,0:T(2,128)(2,1)}), bf16[8,2,122880]{2,1,0:T(2,128)(2,1)}, u32[]{:S(2)}, u32[]{:S(2)}) %all-to-all-start.5) | async-done | bytes 3932192 | tf_op jit(solution)/shard_map/all_to_all | solution.py:59
  552.5 8.5 %reshape.226 = bf16[1920,1,1024]{2,1,0:T(2,128)(2,1)} reshape(bf16[8,2,122880]{2,1,0:T(2,128)(2,1)} %all-to-all-done.5) | data formatting | bytes 7864320
  561.0 6.8 %copy.44 = bf16[1,1920,1024]{2,1,0:T(8,128)(2,1)} copy(bf16[1,1920,1024]{2,0,1:T(2,128)(2,1)} %bitcast.63) | data formatting | bytes 7864320
  567.8 9.7 %gather_fusion = bf16[1536,1024]{1,0:T(8,128)(2,1)S(1)} fusion(bf16[1920,1024]{1,0:T(8,128)(2,1)} %bitcast.60, s32[2048]{0:T(1024)S(1)} %pad_clamp_fusion), kind=kCustom, calls=%fused_computation.1 | custom fusion | bytes 6297600 | tf_op jit(solution)/shard_map/gather | solution.py:60
  577.5 4.4 reshape.190
  581.9 7.9 %multiply_reduce_fusion = bf16[384,1024]{1,0:T(8,128)(2,1)} fusion(f32[384,4,1024]{2,1,0:T(4,128)} %reshape.190, f32[384,4]{1,0:T(8,128)S(1)} %copy.35), kind=kLoop, calls=%fused_computation.6 | loop fusion | flops 2752512 | bytes 7084032 | tf_op jit(solution)/shard_map/reduce_sum | solution.py:62
  589.8 1.3 copy.49
  591.1 3.0 copy.50
  (24 shorter events, 0.2 us)
Async XLA Ops:
  14.0 6.5 %copy-start.4 = (s32[384,4]{0,1:T(4,128)S(1)}, s32[384,4]{0,1:T(4,128)}, u32[]{:S(2)}) copy-start(s32[384,4]{0,1:T(4,128)} %param.8) | copy-start | bytes 18436
  14.0 55.5 %all-to-all-start = ((bf16[8,256,512]{2,1,0:T(8,128)(2,1)}), bf16[8,256,512]{2,1,0:T(8,128)(2,1)S(1)}, u32[]{:S(2)}, u32[]{:S(2)}) async-start(bf16[8,256,512]{2,1,0:T(8,128)(2,1)} %get-tuple-element.17), calls=%async_computation | async-start | bytes 4194304 | tf_op jit(solution)/shard_map/all_to_all | solution.py:17
  69.5 182.6 %copy-start.2 = (bf16[8,256,512]{2,1,0:T(8,128)(2,1)}, bf16[8,256,512]{2,1,0:T(8,128)(2,1)S(1)}, u32[]{:S(2)}) copy-start(bf16[8,256,512]{2,1,0:T(8,128)(2,1)S(1)} %all-to-all-done) | copy-start | bytes 6291460
  247.7 53.4 %all-to-all-start.1 = ((bf16[8,256,512]{2,1,0:T(8,128)(2,1)}), bf16[8,256,512]{2,1,0:T(8,128)(2,1)}, u32[]{:S(2)}, u32[]{:S(2)}) async-start(bf16[8,256,512]{2,1,0:T(8,128)(2,1)} %get-tuple-element.16), calls=%async_computation.1 | async-start | bytes 4194304 | tf_op jit(solution)/shard_map/all_to_all | solution.py:18
  252.1 141.5 %all-gather.3.cloned.1.call-start = ((), (), s32[]{:S(2)}) async-start(), calls=%async_computation.6 | async-start | bytes 5898240 | tf_op jit(solution)/shard_map/all_gather | solution.py:50
  367.1 1.3 copy-start
  389.4 69.9 %all-to-all-start.3 = ((bf16[2,2,262144]{2,1,0:T(2,128)(2,1)}), bf16[2,2,262144]{2,1,0:T(2,128)(2,1)S(1)}, u32[]{:S(2)}, u32[]{:S(2)}) async-start(bf16[2,2,262144]{2,1,0:T(2,128)(2,1)} %reshape.227), calls=%async_computation.3 | async-start | bytes 4194304 | tf_op jit(solution)/shard_map/all_to_all | solution.py:21
  393.6 4.2 copy-start.1
  393.6 4.2 copy-start.6
  459.3 4.9 copy-start.5
  459.3 93.2 %all-to-all-start.5 = ((bf16[8,2,122880]{2,1,0:T(2,128)(2,1)}), bf16[8,2,122880]{2,1,0:T(2,128)(2,1)}, u32[]{:S(2)}, u32[]{:S(2)}) async-start(bf16[8,2,122880]{2,1,0:T(2,128)(2,1)} %reshape.225), calls=%async_computation.5 | async-start | bytes 7864320 | tf_op jit(solution)/shard_map/all_to_all | solution.py:59
  581.9 7.9 %copy-start.3 = (bf16[8,256,512]{2,1,0:T(8,128)(2,1)S(1)}, bf16[8,256,512]{2,1,0:T(8,128)(2,1)}, u32[]{:S(2)}) copy-start(bf16[8,256,512]{2,1,0:T(8,128)(2,1)} %copy-done.2) | copy-start | bytes 6291460
Sparse Core Ops, SparseCore 0:
  313.0 52.6 all-gather.2
where the time goes:
time: 605 us; the launch traced here: 601 us
  blocking collectives  230 us (38%)
  local copies, waits for them, and re-layouts  125 us (21%)
  waiting for transfers between devices  122 us (20%)
  other arithmetic  62.4 us (10%)
  matrix products  27.7 us (5%)
  starting transfers between devices  19.9 us (3%)
  between operations  14.4 us (2%)
    all_to_all x1, blocking collectives, shards(): lax.all_to_all(outbox.reshape(experts, capacity, width), 'fs', split_axis...  178 us
    all_to_all x1, waiting for transfers between devices, shards(): back = lax.all_to_all(summed, 'fs', split_axis=1, concat_axis=0, tiled=True)  75.6 us
    all_to_all x1, blocking collectives, shards(): lax.all_to_all(down_cast, 'fs', split_axis=0, concat_axis=1, tiled=True)  51.7 us
    unnamed x26, local copies, waits for them, and re-layouts  41.9 us
    all_to_all x1, waiting for transfers between devices, shards(): lax.all_to_all(up_cast, 'fs', split_axis=0, concat_axis=1, tiled=True)  39.5 us
    unnamed x3, other arithmetic  37.4 us
    scatter x1, local copies, waits for them, and re-layouts, shards(): jnp.zeros((experts * capacity, width), jnp.bfloat16).at[target]  33 us
    convert_element_type x1, local copies, waits for them, and re-layouts, shards(): summed = total.astype(jnp.bfloat16)  27 us
  transfers between devices with their start and end apart: 5, of which 3 were waited for; matrix products, arithmetic and copies ran while one was open for 25% of the time, Pallas kernels for 0%

commit v1 on v0

--- a/solution.py
+++ b/solution.py
@@ -56,7 +56,10 @@
         ).astype(jnp.bfloat16)
         total = total + part.astype(jnp.float32)
     summed = total.astype(jnp.bfloat16)
-    back = lax.all_to_all(summed, "fs", split_axis=1, concat_axis=0, tiled=True)
+    back = jnp.concatenate(
+        lax.all_to_all(jnp.stack(jnp.split(summed, lax.axis_size("fs"), axis=1)), "fs", 0, 0),
+        axis=0,
+    )
     picked = back.reshape(experts * capacity, quarter)[target].astype(jnp.float32)
     weighted = picked.reshape(tok_rows, TOP, quarter) * route_weight[:, :, None]
     mixed = jnp.sum(weighted, axis=1).astype(jnp.bfloat16)

time: 605 us -> 548 us (0.906)
  local copies, waits for them, and re-layouts: 125 us -> 81.6 us
  other arithmetic: 62.4 us -> 37.6 us
  waiting for transfers between devices: 122 us -> 134 us
    convert_element_type x1 -> x0, local copies, waits for them, and re-layouts: 27 us -> none  [shards(): summed = total.astype(jnp.bfloat16)]
    unnamed x3 -> x2, other arithmetic: 37.4 us -> 12.9 us
    unnamed x26 -> x30, local copies, waits for them, and re-layouts: 41.9 us -> 24.8 us
    all_to_all x1, waiting for transfers between devices: 0.01 us -> 11.5 us  [shards(): lax.all_to_all(down_rows, 'tp', split_axis=1, concat_axis=2, tiled=True)]
  transfers between devices with their start and end apart: 5 -> 5, of which waited for: 3 -> 4; matrix products, arithmetic and copies ran while one was open for 25% -> 19% of each run, Pallas kernels for 0% -> 0%
where the time goes in v1:
time: 548 us; the launch traced here: 544 us
  blocking collectives  230 us (42%)
  waiting for transfers between devices  134 us (24%)
  local copies, waits for them, and re-layouts  81.6 us (15%)
  other arithmetic  37.6 us (7%)
  matrix products  27.6 us (5%)
  starting transfers between devices  19.4 us (4%)
  between operations  14.5 us (3%)
    all_to_all x1, blocking collectives, shards(): lax.all_to_all(outbox.reshape(experts, capacity, width), 'fs', split_axis...  178 us
    all_to_all x1, waiting for transfers between devices, shards(): lax.all_to_all(jnp.stack(jnp.split(summed, lax.axis_size('fs'), axis=1)),...  75.6 us
    all_to_all x1, blocking collectives, shards(): lax.all_to_all(down_cast, 'fs', split_axis=0, concat_axis=1, tiled=True)  51.6 us
    all_to_all x1, waiting for transfers between devices, shards(): lax.all_to_all(up_cast, 'fs', split_axis=0, concat_axis=1, tiled=True)  39.5 us
    scatter x1, local copies, waits for them, and re-layouts, shards(): jnp.zeros((experts * capacity, width), jnp.bfloat16).at[target]  33.3 us
    unnamed x30, local copies, waits for them, and re-layouts  24.8 us
    unnamed x2, other arithmetic  12.9 us
    dot_general x1, matrix products, shards(): jnp.einsum('erd,edf->erf', inbox, up_mine, preferred_element_type=jnp.flo...  11.7 us
  transfers between devices with their start and end apart: 5, of which 4 were waited for; matrix products, arithmetic and copies ran while one was open for 19% of the time, Pallas kernels for 0%

profile of v1, /device:TPU:0, one launch (start us, length us, event | category | flops | bytes accessed | tf_op | source)
XLA Modules:
  0.0 544.3 jit_solution(15226786300977752887)
XLA Ops:
  7.2 6.8 %multiply_convert_fusion = (bf16[8,256,512]{2,1,0:T(8,128)(2,1)}, bf16[8,256,512]{2,1,0:T(8,128)(2,1)}) fusion(f32[8,256,512]{2,1,0:T(8,128)} %param.12, f32[256]{0:T(256)} %param.10, f32[8,256,512]{2,1,0:T(8,128)} %param.11), kind=kLoop, calls=%fused_computation.7 | loop fusion | flops 4194304 | bytes 12583936 | tf_op jit(solution)/shard_map/convert_element_type | solution.py:14
  14.0 6.5 %all-to-all-start = ((bf16[8,256,512]{2,1,0:T(8,128)(2,1)}), bf16[8,256,512]{2,1,0:T(8,128)(2,1)S(1)}, u32[]{:S(2)}, u32[]{:S(2)}) async-start(bf16[8,256,512]{2,1,0:T(8,128)(2,1)} %get-tuple-element.17), calls=%async_computation | async-start | bytes 4194304 | tf_op jit(solution)/shard_map/all_to_all | solution.py:17
  20.6 0.1 eq.29
  20.9 2.3 reduce-window.6
  23.2 0.3 slice_reduce_fusion
  23.5 0.2 reduce-window.9
  23.7 0.1 copy.30
  23.8 0.2 mul.72
  24.0 0.3 fusion.20
  24.5 1.8 fusion.4
  26.3 2.9 fusion.5
  29.2 33.3 %scatter_custom_fusion = bf16[1920,2048]{1,0:T(8,128)(2,1)} fusion(s32[1536]{0:T(1024)S(1)} %fusion.19, bf16[384,2048]{1,0:T(8,128)(2,1)} %fusion.5, s32[2048]{0:T(1024)S(1)} %pad_clamp_fusion.1, bf16[]{:T(256)} %constant.17.clone.1), kind=kCustom, calls=%fused_computation.4 | custom fusion | bytes 7864832 | tf_op jit(solution)/shard_map/scatter | solution.py:38
  62.5 7.0 %all-to-all-done = bf16[8,256,512]{2,1,0:T(8,128)(2,1)S(1)} async-done(((bf16[8,256,512]{2,1,0:T(8,128)(2,1)}), bf16[8,256,512]{2,1,0:T(8,128)(2,1)S(1)}, u32[]{:S(2)}, u32[]{:S(2)}) %all-to-all-start) | async-done | bytes 2097184 | tf_op jit(solution)/shard_map/all_to_all | solution.py:17
  69.5 178.2 %all_to_all.68 = bf16[8,240,2048]{2,1,0:T(8,128)(2,1)} all-to-all(bf16[8,240,2048]{2,1,0:T(8,128)(2,1)} %bitcast.86), channel_id=1, replica_groups=mesh['grp'=2,'fs'=8,'tp'=2] {'fs'}, dimensions={0} | all-to-all | bytes 15728640 | tf_op jit(solution)/shard_map/all_to_all | solution.py:39
  247.7 4.3 all-to-all-start.1
  252.1 9.5 %fusion.21 = f32[1920,512]{1,0:T(8,128)} fusion(bf16[1920,2048]{1,0:T(8,128)(2,1)} %bitcast.96, bf16[2048,512]{1,0:T(8,128)(2,1)S(1)} %bitcast.93), kind=kOutput, calls=%fused_computation.59 | convolution fusion | flops 4026531840 | bytes 13893632 | tf_op jit(solution)/shard_map/erd,edf->erf/dot_general | solution.py:42
  261.6 39.5 %all-to-all-done.1 = bf16[8,256,512]{2,1,0:T(8,128)(2,1)} async-done(((bf16[8,256,512]{2,1,0:T(8,128)(2,1)}), bf16[8,256,512]{2,1,0:T(8,128)(2,1)}, u32[]{:S(2)}, u32[]{:S(2)}) %all-to-all-start.1) | async-done | bytes 2097184 | tf_op jit(solution)/shard_map/all_to_all | solution.py:18
  301.1 11.7 %multiply_convert_fusion.2 = bf16[1920,512]{1,0:T(8,128)(2,1)} fusion(f32[1920,512]{1,0:T(8,128)} %fusion.21, bf16[1920,2048]{1,0:T(8,128)(2,1)} %bitcast.97, bf16[2048,512]{1,0:T(8,128)(2,1)} %bitcast.8), kind=kOutput, calls=%fused_computation.10 | convolution fusion | flops 4036362240 | bytes 15859712 | tf_op jit(solution)/shard_map/erd,edf->erf/dot_general | solution.py:43
  312.8 2.5 convert_element_type.62
  315.3 51.6 %all_to_all.69 = bf16[8,128,1024]{2,1,0:T(8,128)(2,1)S(1)} all-to-all(bf16[8,128,1024]{2,1,0:T(8,128)(2,1)S(1)} %convert_element_type.62), channel_id=1, replica_groups=mesh['grp'=2,'fs'=8,'tp'=2] {'fs'}, dimensions={0} | all-to-all | bytes 4194304 | tf_op jit(solution)/shard_map/all_to_all | solution.py:20
  367.0 1.3 copy-done
  368.3 5.2 copy.39
  373.4 0.5 broadcast.146
  373.9 12.8 %reduce.6 = bf16[1024,1024]{1,0:T(8,128)(2,1)S(1)} reduce(bf16[1024,1,1024]{2,1,0:T(2,128)(2,1)} %bitcast.87, bf16[]{:T(256)} %broadcast.146), dimensions={1}, to_apply=%bitcast.84.reduce_sub_computation | reduce | bytes 4194306
  386.7 2.5 reshape.217
  389.2 3.8 all-to-all-start.3
  393.1 4.2 fusion.6
  397.3 2.3 fusion.2
  399.6 0.9 fusion.14
  400.4 0.8 fusion.13
  401.3 0.8 fusion.12
  402.1 0.8 fusion.11
  402.9 0.8 fusion.10
  403.7 0.8 fusion.9
  404.6 0.8 fusion.8
  405.4 0.8 fusion.7
  406.2 11.5 %all-to-all-done.3 = bf16[2,2,262144]{2,1,0:T(2,128)(2,1)S(1)} async-done(((bf16[2,2,262144]{2,1,0:T(2,128)(2,1)}), bf16[2,2,262144]{2,1,0:T(2,128)(2,1)S(1)}, u32[]{:S(2)}, u32[]{:S(2)}) %all-to-all-start.3) | async-done | bytes 2097184 | tf_op jit(solution)/shard_map/all_to_all | solution.py:21
  417.7 4.7 all-to-all-start.5
  422.6 3.1 reshape.218
  425.7 3.0 copy.35
  428.7 2.6 copy.29
  431.3 3.9 copy.34
  435.2 75.6 %all-to-all-done.5 = bf16[8,1,240,1024]{3,2,1,0:T(8,128)(2,1)} async-done(((bf16[8,1,240,1024]{3,2,1,0:T(8,128)(2,1)}), bf16[8,1,240,1024]{3,2,1,0:T(8,128)(2,1)}, u32[]{:S(2)}, u32[]{:S(2)}) %all-to-all-start.5) | async-done | bytes 3932192 | tf_op jit(solution)/shard_map/all_to_all | solution.py:60
  510.8 9.7 %gather_fusion = bf16[1536,1024]{1,0:T(8,128)(2,1)S(1)} fusion(bf16[1920,1024]{1,0:T(8,128)(2,1)} %bitcast.24, s32[2048]{0:T(1024)S(1)} %pad_clamp_fusion), kind=kCustom, calls=%fused_computation.1 | custom fusion | bytes 6297600 | tf_op jit(solution)/shard_map/gather | solution.py:63
  520.6 4.4 reshape.182
  524.9 7.9 %multiply_reduce_fusion = bf16[384,1024]{1,0:T(8,128)(2,1)} fusion(f32[384,4,1024]{2,1,0:T(4,128)} %reshape.182, f32[384,4]{1,0:T(8,128)S(1)} %copy.33), kind=kLoop, calls=%fused_computation.6 | loop fusion | flops 2752512 | bytes 7084032 | tf_op jit(solution)/shard_map/reduce_sum | solution.py:65
  532.8 1.3 copy.49
  534.1 3.0 copy.50
  (27 shorter events, 0.7 us)
Async XLA Ops:
  14.0 6.5 %copy-start.4 = (s32[384,4]{0,1:T(4,128)S(1)}, s32[384,4]{0,1:T(4,128)}, u32[]{:S(2)}) copy-start(s32[384,4]{0,1:T(4,128)} %param.8) | copy-start | bytes 18436
  14.0 55.5 %all-to-all-start = ((bf16[8,256,512]{2,1,0:T(8,128)(2,1)}), bf16[8,256,512]{2,1,0:T(8,128)(2,1)S(1)}, u32[]{:S(2)}, u32[]{:S(2)}) async-start(bf16[8,256,512]{2,1,0:T(8,128)(2,1)} %get-tuple-element.17), calls=%async_computation | async-start | bytes 4194304 | tf_op jit(solution)/shard_map/all_to_all | solution.py:17
  69.5 182.6 %copy-start.2 = (bf16[8,256,512]{2,1,0:T(8,128)(2,1)}, bf16[8,256,512]{2,1,0:T(8,128)(2,1)S(1)}, u32[]{:S(2)}) copy-start(bf16[8,256,512]{2,1,0:T(8,128)(2,1)S(1)} %all-to-all-done) | copy-start | bytes 6291460
  247.7 53.4 %all-to-all-start.1 = ((bf16[8,256,512]{2,1,0:T(8,128)(2,1)}), bf16[8,256,512]{2,1,0:T(8,128)(2,1)}, u32[]{:S(2)}, u32[]{:S(2)}) async-start(bf16[8,256,512]{2,1,0:T(8,128)(2,1)} %get-tuple-element.16), calls=%async_computation.1 | async-start | bytes 4194304 | tf_op jit(solution)/shard_map/all_to_all | solution.py:18
  252.1 141.0 %all-gather.3.cloned.1.call-start = ((), (), s32[]{:S(2)}) async-start(), calls=%async_computation.6 | async-start | bytes 5898240 | tf_op jit(solution)/shard_map/all_gather | solution.py:50
  367.0 1.3 copy-start
  389.2 28.5 %all-to-all-start.3 = ((bf16[2,2,262144]{2,1,0:T(2,128)(2,1)}), bf16[2,2,262144]{2,1,0:T(2,128)(2,1)S(1)}, u32[]{:S(2)}, u32[]{:S(2)}) async-start(bf16[2,2,262144]{2,1,0:T(2,128)(2,1)} %reshape.217), calls=%async_computation.3 | async-start | bytes 4194304 | tf_op jit(solution)/shard_map/all_to_all | solution.py:21
  393.0 4.2 copy-start.1
  393.1 4.2 copy-start.6
  406.2 16.3 %copy-start.5 = (f32[384,4]{0,1:T(4,128)S(1)}, f32[384,4]{0,1:T(4,128)}, u32[]{:S(2)}) copy-start(f32[384,4]{0,1:T(4,128)} %param.9) | copy-start | bytes 18436
  417.7 93.1 %all-to-all-start.5 = ((bf16[8,1,240,1024]{3,2,1,0:T(8,128)(2,1)}), bf16[8,1,240,1024]{3,2,1,0:T(8,128)(2,1)}, u32[]{:S(2)}, u32[]{:S(2)}) async-start(bf16[8,1,240,1024]{3,2,1,0:T(8,128)(2,1)} %fusion.7), calls=%async_computation.5 | async-start | bytes 7864320 | tf_op jit(solution)/shard_map/all_to_all | solution.py:60
  524.9 7.9 %copy-start.3 = (bf16[8,256,512]{2,1,0:T(8,128)(2,1)S(1)}, bf16[8,256,512]{2,1,0:T(8,128)(2,1)}, u32[]{:S(2)}) copy-start(bf16[8,256,512]{2,1,0:T(8,128)(2,1)} %copy-done.2) | copy-start | bytes 6291460
Sparse Core Ops, SparseCore 0:
  312.9 52.6 all-gather.2
